TPU v7x, 32 devices: a whole 2x2x4 slice. The times are simulated.
32 devices in a mesh: pp: 2 (over x), fs: 4 (over y, core), tp: 4 (over z).
Axes of the slice: x: 2, y: 2, z: 4, core: 2. Of those that a mesh axis runs over, the one named last changes fastest.
Arguments:
- inputs: bfloat16 [512, 2048], P('pp', ('fs', 'tp')), may hold values from -6 to 6
- norm_gain: bfloat16 [2, 2048], P('pp', ('fs', 'tp')), may hold values from 0.099609375 to 1.8984375
- w_value: bfloat16 [2, 2048, 2048], P('pp', None, ('fs', 'tp')), may hold values from -0.125 to 0.125
- w_gate: bfloat16 [2, 2048, 2048], P('pp', None, ('fs', 'tp')), may hold values from -0.125 to 0.125
- w_taps: bfloat16 [2, 31, 2048], P('pp', None, ('fs', 'tp')), may hold values from -1 to 1
- ln_gain: float32 [2, 2048], P('pp', ('fs', 'tp')), may hold values from 0.1 to 1.9
- ln_shift: float32 [2, 2048], P('pp', ('fs', 'tp')), may hold values from -3 to 3
Outputs:
- outputs: bfloat16 [512, 2048], P('pp', ('fs', 'tp'))
All inputs are finite; a program needn't handle non-finite values.
Results may differ from a plain program's by a relative error of at most 0.0085.
Values may be sent and summed in bfloat16 or wider, within the bound.
A program may use at most 64 MiB of HBM per device.

v0:
```python
import jax
import jax.numpy as jnp
from jax import lax
from jax.sharding import PartitionSpec as P

LEN = 128
norm_eps = 1e-06
layer_eps = 1e-05


def from_behind(block, axis, distance):
    devices = range(lax.axis_size(axis))
    route = [(i - distance, i) for i in devices if i - distance in devices]
    return lax.ppermute(block, axis, route)


def local(inputs, norm_gain, w_value, w_gate, w_taps, ln_gain, ln_shift):
    num_sections = lax.axis_size("pp")
    my_section = lax.axis_index("pp")
    model_width = w_value.shape[1]
    channels = w_value.shape[2]
    tap_count = w_taps.shape[1]
    fed_rows = lax.all_gather(inputs, "pp", axis=0, tiled=True)
    total_rows = fed_rows.shape[0]
    block_rows = LEN
    per_batch = LEN // block_rows
    block_count = total_rows // block_rows
    step_count = block_count + num_sections - 1
    gain_row = norm_gain[0]
    value_weight = w_value[0]
    gate_weight = w_gate[0]
    tap_weights = w_taps[0].astype(jnp.float32)
    layer_gain = ln_gain[0]
    layer_shift = ln_shift[0]

    def convolve(operands):
        history, gated_rows = operands
        padded = jnp.concatenate([history, gated_rows], axis=0)
        convolved = jnp.zeros((block_rows, channels), jnp.float32)
        for tap_index in range(tap_count):
            convolved = (
                convolved + padded[tap_index : tap_index + block_rows] * tap_weights[tap_index]
            )
        return convolved

    def skip_convolve(operands):
        return jnp.zeros((block_rows, channels), jnp.float32)

    def process_block(stream, history, active):
        stream_f = stream.astype(jnp.float32)
        zero_block = jnp.zeros((block_rows, channels), jnp.float32)
        squares = lax.psum(jnp.sum(stream_f * stream_f, axis=1), ("fs", "tp"))
        scale_rows = lax.rsqrt(squares / model_width + norm_eps)[:, None]
        normed = (stream_f * scale_rows * gain_row.astype(jnp.float32)).astype(jnp.bfloat16)
        shard_piece = lax.all_gather(normed, ("fs", "tp"), axis=1, tiled=True)

        def accumulate(current):
            return (
                jnp.dot(shard_piece, value_weight, preferred_element_type=jnp.float32),
                jnp.dot(shard_piece, gate_weight, preferred_element_type=jnp.float32),
            )

        def unchanged(current):
            return current

        value_sum, gate_sum = lax.cond(active, accumulate, unchanged, (zero_block, zero_block))
        gated_rows = value_sum * jax.nn.sigmoid(gate_sum)
        convolved = lax.cond(active, convolve, skip_convolve, (history, gated_rows))
        new_history = jnp.where(
            active, jnp.concatenate([history, gated_rows], axis=0)[block_rows:], history
        )
        moments = lax.psum(
            (jnp.sum(convolved, axis=1), jnp.sum(convolved * convolved, axis=1)), ("fs", "tp")
        )
        row_mean = moments[0][:, None] / model_width
        row_var = moments[1][:, None] / model_width - row_mean * row_mean
        normed_conv = (convolved - row_mean) * lax.rsqrt(
            row_var + layer_eps
        ) * layer_gain + layer_shift
        new_stream = (stream_f + jax.nn.silu(normed_conv)).astype(jnp.bfloat16)
        return (jnp.where(active, new_stream, stream), new_history)

    def step_body(step_index, loop_state):
        stream, history, results = loop_state
        block_index = step_index - my_section
        active = (block_index >= 0) & (block_index < block_count)
        safe_index = jnp.clip(block_index, 0, block_count - 1)
        row_offset = safe_index * block_rows
        first_rows = lax.dynamic_slice_in_dim(fed_rows, row_offset, block_rows, 0)
        stream = jnp.where(my_section == 0, first_rows, stream)
        history = jnp.where(
            active & (safe_index % per_batch == 0), jnp.zeros_like(history), history
        )
        new_stream, new_history = process_block(stream, history, active)
        previous = lax.dynamic_slice_in_dim(results, row_offset, block_rows, 0)
        keep_rows = active & (my_section == num_sections - 1)
        results = lax.dynamic_update_slice_in_dim(
            results, jnp.where(keep_rows, new_stream, previous), row_offset, 0
        )
        passed = from_behind(new_stream, "pp", 1)
        return (passed, new_history, results)

    initial = (
        jnp.zeros((block_rows, channels), jnp.bfloat16),
        jnp.zeros((tap_count - 1, channels), jnp.float32),
        jnp.zeros((total_rows, channels), jnp.bfloat16),
    )
    final_state = lax.fori_loop(0, step_count, step_body, initial)
    own_rows = inputs.shape[0]
    shares = final_state[2].reshape(num_sections, own_rows, channels)
    arrived = lax.all_to_all(shares, "pp", split_axis=0, concat_axis=0, tiled=True)
    return arrived[num_sections - 1]


def solution(mesh):
    in_specs = (
        P("pp", ("fs", "tp")),
        P("pp", ("fs", "tp")),
        P("pp", None, ("fs", "tp")),
        P("pp", None, ("fs", "tp")),
        P("pp", None, ("fs", "tp")),
        P("pp", ("fs", "tp")),
        P("pp", ("fs", "tp")),
    )
    out_specs = P("pp", ("fs", "tp"))
    return jax.shard_map(local, mesh=mesh, in_specs=in_specs, out_specs=out_specs, check_vma=False)
```

profile of v0, /device:TPU:0, one launch (start us, length us, event | category | flops | bytes accessed | tf_op | source)
XLA Modules:
  0.0 539.6 jit_solution(15302463253678728073)
XLA Ops:
  0.0 6.3 %all_gather.13 = bf16[512,128]{1,0:T(8,128)(2,1)S(1)} all-gather(bf16[256,128]{1,0:T(8,128)(2,1)} %param.13), channel_id=1, replica_groups=mesh['pp'=2,'fs'=4,'tp'=4] {'pp'}, dimensions={0}, use_global_device_ids=true | all-gather | bytes 196608 | tf_op jit(solution)/shard_map/all_gather | solution.py:23
  6.3 0.6 copy-done.1
  7.0 524.0 %while.20 = (s32[]{:T(128)}, bf16[128,128]{1,0:T(8,128)(2,1)S(1)}, f32[30,128]{1,0:T(8,128)S(1)}, bf16[512,128]{1,0:T(8,128)(2,1)S(1)}, s32[]{:T(128)}, /*index=...) while((s32[]{:T(128)}, bf16[128,128]{1,0:T(8,128)(2,1)S(1)}, ...), condition=%wide.region_11.12_spmd.clone, body=%wide.region_0.11_spmd.clone.sunk | while | flops 136179984 | bytes 5903558 | solution.py:108
  7.0 0.1 fusion.105
  7.1 33.1 %psum.46 = f32[128]{0:T(128)S(1)} all-reduce(f32[128]{0:T(128)S(1)} %get-tuple-element.554), channel_id=1, replica_groups=mesh['pp'=2,'fs'=4,'tp'=4] {'fs','tp'}, use_global_device_ids=true, to_apply=%region_2.2 | all-reduce | flops 128 | bytes 1024 | tf_op jit(solution)/shard_map/while/body/eval_jaxpr/psum | solution.py:52
  40.3 33.2 %all_gather.16 = bf16[128,2048]{1,0:T(8,128)(2,1)S(1)} all-gather(bf16[128,128]{1,0:T(8,128)(2,1)S(1)} %fusion.106), channel_id=1, replica_groups=mesh['pp'=2,'fs'=4,'tp'=4] {'fs','tp'}, dimensions={1}, use_global_device_ids=true | all-gather | bytes 557056 | tf_op jit(solution)/shard_map/while/body/eval_jaxpr/all_gather | solution.py:55
  73.5 1.6 conditional.6
  73.5 1.3 fusion
  74.9 0.3 fusion.97
  75.2 0.3 conditional.7
  75.3 0.2 fusion.5
  75.5 0.1 fusion.107
  75.6 31.4 %all-reduce.2 = (f32[128]{0:T(128)S(1)}, f32[128]{0:T(128)S(1)}) all-reduce(f32[128]{0:T(128)S(1)} %get-tuple-element.558, f32[128]{0:T(128)S(1)} %get-tuple-element.559), channel_id=1, replica_groups=mesh['pp'=2,'fs'=4,'tp'=4] {'fs','tp'}, use_global_device_ids=true, to_apply=%region_10.10 | all-reduce | flops 256 | bytes 2048 | tf_op jit(solution)/shard_map/while/body/eval_jaxpr/psum | solution.py:72
  107.0 0.1 select_dynamic-update-slice_fusion.2
  107.1 1.7 collective-permute-start
  108.8 1.6 collective-permute-done
  110.4 0.1 fusion.105
  110.5 30.2 %psum.46 = f32[128]{0:T(128)S(1)} all-reduce(f32[128]{0:T(128)S(1)} %get-tuple-element.554), channel_id=1, replica_groups=mesh['pp'=2,'fs'=4,'tp'=4] {'fs','tp'}, use_global_device_ids=true, to_apply=%region_2.2 | all-reduce | flops 128 | bytes 1024 | tf_op jit(solution)/shard_map/while/body/eval_jaxpr/psum | solution.py:52
  140.8 36.4 %all_gather.16 = bf16[128,2048]{1,0:T(8,128)(2,1)S(1)} all-gather(bf16[128,128]{1,0:T(8,128)(2,1)S(1)} %fusion.106), channel_id=1, replica_groups=mesh['pp'=2,'fs'=4,'tp'=4] {'fs','tp'}, dimensions={1}, use_global_device_ids=true | all-gather | bytes 557056 | tf_op jit(solution)/shard_map/while/body/eval_jaxpr/all_gather | solution.py:55
  177.2 1.6 conditional.6
  177.2 1.3 fusion
  178.5 0.3 fusion.97
  178.8 0.3 conditional.7
  178.9 0.2 fusion.5
  179.1 0.1 fusion.107
  179.2 29.7 %all-reduce.2 = (f32[128]{0:T(128)S(1)}, f32[128]{0:T(128)S(1)}) all-reduce(f32[128]{0:T(128)S(1)} %get-tuple-element.558, f32[128]{0:T(128)S(1)} %get-tuple-element.559), channel_id=1, replica_groups=mesh['pp'=2,'fs'=4,'tp'=4] {'fs','tp'}, use_global_device_ids=true, to_apply=%region_10.10 | all-reduce | flops 256 | bytes 2048 | tf_op jit(solution)/shard_map/while/body/eval_jaxpr/psum | solution.py:72
  208.9 0.1 select_dynamic-update-slice_fusion.2
  209.1 4.2 collective-permute-start
  213.3 1.6 collective-permute-done
  214.9 0.1 fusion.105
  215.0 32.0 %psum.46 = f32[128]{0:T(128)S(1)} all-reduce(f32[128]{0:T(128)S(1)} %get-tuple-element.554), channel_id=1, replica_groups=mesh['pp'=2,'fs'=4,'tp'=4] {'fs','tp'}, use_global_device_ids=true, to_apply=%region_2.2 | all-reduce | flops 128 | bytes 1024 | tf_op jit(solution)/shard_map/while/body/eval_jaxpr/psum | solution.py:52
  247.1 33.5 %all_gather.16 = bf16[128,2048]{1,0:T(8,128)(2,1)S(1)} all-gather(bf16[128,128]{1,0:T(8,128)(2,1)S(1)} %fusion.106), channel_id=1, replica_groups=mesh['pp'=2,'fs'=4,'tp'=4] {'fs','tp'}, dimensions={1}, use_global_device_ids=true | all-gather | bytes 557056 | tf_op jit(solution)/shard_map/while/body/eval_jaxpr/all_gather | solution.py:55
  280.6 1.6 conditional.6
  280.6 1.3 fusion
  282.0 0.3 fusion.97
  282.3 0.3 conditional.7
  282.4 0.2 fusion.5
  282.6 0.1 fusion.107
  282.7 32.0 %all-reduce.2 = (f32[128]{0:T(128)S(1)}, f32[128]{0:T(128)S(1)}) all-reduce(f32[128]{0:T(128)S(1)} %get-tuple-element.558, f32[128]{0:T(128)S(1)} %get-tuple-element.559), channel_id=1, replica_groups=mesh['pp'=2,'fs'=4,'tp'=4] {'fs','tp'}, use_global_device_ids=true, to_apply=%region_10.10 | all-reduce | flops 256 | bytes 2048 | tf_op jit(solution)/shard_map/while/body/eval_jaxpr/psum | solution.py:72
  314.7 0.1 select_dynamic-update-slice_fusion.2
  314.8 4.2 collective-permute-start
  319.1 1.6 collective-permute-done
  320.6 0.1 fusion.105
  320.8 29.8 %psum.46 = f32[128]{0:T(128)S(1)} all-reduce(f32[128]{0:T(128)S(1)} %get-tuple-element.554), channel_id=1, replica_groups=mesh['pp'=2,'fs'=4,'tp'=4] {'fs','tp'}, use_global_device_ids=true, to_apply=%region_2.2 | all-reduce | flops 128 | bytes 1024 | tf_op jit(solution)/shard_map/while/body/eval_jaxpr/psum | solution.py:52
  350.7 36.8 %all_gather.16 = bf16[128,2048]{1,0:T(8,128)(2,1)S(1)} all-gather(bf16[128,128]{1,0:T(8,128)(2,1)S(1)} %fusion.106), channel_id=1, replica_groups=mesh['pp'=2,'fs'=4,'tp'=4] {'fs','tp'}, dimensions={1}, use_global_device_ids=true | all-gather | bytes 557056 | tf_op jit(solution)/shard_map/while/body/eval_jaxpr/all_gather | solution.py:55
  387.5 1.6 conditional.6
  387.5 1.3 fusion
  388.9 0.3 fusion.97
  389.2 0.3 conditional.7
  389.3 0.2 fusion.5
  389.5 0.1 fusion.107
  389.6 29.7 %all-reduce.2 = (f32[128]{0:T(128)S(1)}, f32[128]{0:T(128)S(1)}) all-reduce(f32[128]{0:T(128)S(1)} %get-tuple-element.558, f32[128]{0:T(128)S(1)} %get-tuple-element.559), channel_id=1, replica_groups=mesh['pp'=2,'fs'=4,'tp'=4] {'fs','tp'}, use_global_device_ids=true, to_apply=%region_10.10 | all-reduce | flops 256 | bytes 2048 | tf_op jit(solution)/shard_map/while/body/eval_jaxpr/psum | solution.py:72
  419.3 0.1 select_dynamic-update-slice_fusion.2
  419.5 4.2 collective-permute-start
  423.7 1.6 collective-permute-done
  425.4 32.0 %psum.46 = f32[128]{0:T(128)S(1)} all-reduce(f32[128]{0:T(128)S(1)} %get-tuple-element.554), channel_id=1, replica_groups=mesh['pp'=2,'fs'=4,'tp'=4] {'fs','tp'}, use_global_device_ids=true, to_apply=%region_2.2 | all-reduce | flops 128 | bytes 1024 | tf_op jit(solution)/shard_map/while/body/eval_jaxpr/psum | solution.py:52
  457.5 33.3 %all_gather.16 = bf16[128,2048]{1,0:T(8,128)(2,1)S(1)} all-gather(bf16[128,128]{1,0:T(8,128)(2,1)S(1)} %fusion.106), channel_id=1, replica_groups=mesh['pp'=2,'fs'=4,'tp'=4] {'fs','tp'}, dimensions={1}, use_global_device_ids=true | all-gather | bytes 557056 | tf_op jit(solution)/shard_map/while/body/eval_jaxpr/all_gather | solution.py:55
  490.9 0.1 fusion.107
  491.1 32.0 %all-reduce.2 = (f32[128]{0:T(128)S(1)}, f32[128]{0:T(128)S(1)}) all-reduce(f32[128]{0:T(128)S(1)} %get-tuple-element.558, f32[128]{0:T(128)S(1)} %get-tuple-element.559), channel_id=1, replica_groups=mesh['pp'=2,'fs'=4,'tp'=4] {'fs','tp'}, use_global_device_ids=true, to_apply=%region_10.10 | all-reduce | flops 256 | bytes 2048 | tf_op jit(solution)/shard_map/while/body/eval_jaxpr/psum | solution.py:72
  523.0 0.1 select_dynamic-update-slice_fusion.2
  523.2 6.1 %collective-permute-start = (bf16[128,128]{1,0:T(8,128)(2,1)S(1)}, bf16[128,128]{1,0:T(8,128)(2,1)S(1)}, u32[]{:S(2)}, u32[]{:S(2)}) collective-permute-start(bf16[128,128]{1,0:T(8,128)(2,1)S(1)} %get-tuple-element.564), channel_id=1, source_target_pairs={{0,16},{1,17},{2,18},{3,19},{4,20},{5,21},{6,22},{7,23},{8,24},{9,... | collective-permute-start | bytes 98312 | tf_op jit(solution)/shard_map/while/body/eval_jaxpr/ppermute | solution.py:14
  529.3 1.7 collective-permute-done
  531.0 8.0 %all_to_all.5 = bf16[2,256,128]{2,1,0:T(8,128)(2,1)S(1)} all-to-all(bf16[2,256,128]{2,1,0:T(8,128)(2,1)S(1)} %bitcast.83), channel_id=1, replica_groups=mesh['pp'=2,'fs'=4,'tp'=4] {'pp'}, dimensions={0} | all-to-all | bytes 262144 | tf_op jit(solution)/shard_map/all_to_all | solution.py:111
  539.0 0.6 slice_bitcast_fusion.31
  (65 shorter events, 1.0 us)
Async XLA Ops:
  0.0 6.3 %copy-start.3 = (bf16[1,31,128]{2,1,0:T(8,128)(2,1)S(1)}, bf16[1,31,128]{2,1,0:T(8,128)(2,1)}, u32[]{:S(2)}) copy-start(bf16[1,31,128]{2,1,0:T(8,128)(2,1)} %param.17) | copy-start | bytes 23812
  6.3 0.7 copy-start.1
  6.3 0.7 copy-start.2
  6.3 0.7 copy-start.4
  7.0 66.5 %copy-start = (bf16[2048,128]{1,0:T(8,128)(2,1)S(1)}, bf16[2048,128]{1,0:T(8,128)(2,1)}, u32[]{:S(2)}) copy-start(bf16[2048,128]{1,0:T(8,128)(2,1)} %get-tuple-element.619) | copy-start | bytes 1572868 | tf_op jit(solution)/shard_map/while
  107.1 3.2 collective-permute-start
  110.4 66.8 %copy-start = (bf16[2048,128]{1,0:T(8,128)(2,1)S(1)}, bf16[2048,128]{1,0:T(8,128)(2,1)}, u32[]{:S(2)}) copy-start(bf16[2048,128]{1,0:T(8,128)(2,1)} %get-tuple-element.619) | copy-start | bytes 1572868 | tf_op jit(solution)/shard_map/while
  209.1 5.8 %collective-permute-start = (bf16[128,128]{1,0:T(8,128)(2,1)S(1)}, bf16[128,128]{1,0:T(8,128)(2,1)S(1)}, u32[]{:S(2)}, u32[]{:S(2)}) collective-permute-start(bf16[128,128]{1,0:T(8,128)(2,1)S(1)} %get-tuple-element.564), channel_id=1, source_target_pairs={{0,16},{1,17},{2,18},{3,19},{4,20},{5,21},{6,22},{7,23},{8,24},{9,... | collective-permute-start | bytes 98312 | tf_op jit(solution)/shard_map/while/body/eval_jaxpr/ppermute | solution.py:14
  214.9 65.7 %copy-start = (bf16[2048,128]{1,0:T(8,128)(2,1)S(1)}, bf16[2048,128]{1,0:T(8,128)(2,1)}, u32[]{:S(2)}) copy-start(bf16[2048,128]{1,0:T(8,128)(2,1)} %get-tuple-element.619) | copy-start | bytes 1572868 | tf_op jit(solution)/shard_map/while
  314.8 5.8 %collective-permute-start = (bf16[128,128]{1,0:T(8,128)(2,1)S(1)}, bf16[128,128]{1,0:T(8,128)(2,1)S(1)}, u32[]{:S(2)}, u32[]{:S(2)}) collective-permute-start(bf16[128,128]{1,0:T(8,128)(2,1)S(1)} %get-tuple-element.564), channel_id=1, source_target_pairs={{0,16},{1,17},{2,18},{3,19},{4,20},{5,21},{6,22},{7,23},{8,24},{9,... | collective-permute-start | bytes 98312 | tf_op jit(solution)/shard_map/while/body/eval_jaxpr/ppermute | solution.py:14
  320.6 66.9 %copy-start = (bf16[2048,128]{1,0:T(8,128)(2,1)S(1)}, bf16[2048,128]{1,0:T(8,128)(2,1)}, u32[]{:S(2)}) copy-start(bf16[2048,128]{1,0:T(8,128)(2,1)} %get-tuple-element.619) | copy-start | bytes 1572868 | tf_op jit(solution)/shard_map/while
  419.5 5.8 %collective-permute-start = (bf16[128,128]{1,0:T(8,128)(2,1)S(1)}, bf16[128,128]{1,0:T(8,128)(2,1)S(1)}, u32[]{:S(2)}, u32[]{:S(2)}) collective-permute-start(bf16[128,128]{1,0:T(8,128)(2,1)S(1)} %get-tuple-element.564), channel_id=1, source_target_pairs={{0,16},{1,17},{2,18},{3,19},{4,20},{5,21},{6,22},{7,23},{8,24},{9,... | collective-permute-start | bytes 98312 | tf_op jit(solution)/shard_map/while/body/eval_jaxpr/ppermute | solution.py:14
  425.3 65.6 %copy-start = (bf16[2048,128]{1,0:T(8,128)(2,1)S(1)}, bf16[2048,128]{1,0:T(8,128)(2,1)}, u32[]{:S(2)}) copy-start(bf16[2048,128]{1,0:T(8,128)(2,1)} %get-tuple-element.619) | copy-start | bytes 1572868 | tf_op jit(solution)/shard_map/while
  523.2 7.8 %collective-permute-start = (bf16[128,128]{1,0:T(8,128)(2,1)S(1)}, bf16[128,128]{1,0:T(8,128)(2,1)S(1)}, u32[]{:S(2)}, u32[]{:S(2)}) collective-permute-start(bf16[128,128]{1,0:T(8,128)(2,1)S(1)} %get-tuple-element.564), channel_id=1, source_target_pairs={{0,16},{1,17},{2,18},{3,19},{4,20},{5,21},{6,22},{7,23},{8,24},{9,... | collective-permute-start | bytes 98312 | tf_op jit(solution)/shard_map/while/body/eval_jaxpr/ppermute | solution.py:14
where the time goes:
time: 540 us
  blocking collectives  499 us (92%)
  starting transfers between devices  20.4 us (4%)
  waiting for transfers between devices  8.02 us (1%)
  matrix products  6.45 us (1%)
    all_gather x5, blocking collectives, process_block(): shard_piece = lax.all_gather(normed, ('fs', 'tp'), axis=1, tiled=True)  173 us
    psum x5, blocking collectives, process_block(): squares = lax.psum(jnp.sum(stream_f * stream_f, axis=1), ('fs', 'tp'))  157 us
    psum x5, blocking collectives, process_block(): lax.psum((jnp.sum(convolved, axis=1), jnp.sum(convolved * convolved, axis...  155 us
    ppermute x5, starting transfers between devices, from_behind(): return lax.ppermute(block, axis, route)  20.4 us
  transfers between devices with their start and end apart: 5, of which 5 were waited for; matrix products, arithmetic and copies ran while one was open for 0% of the time, Pallas kernels for 0%

commit v1 on v0

--- a/solution.py
+++ b/solution.py
@@ -70,7 +70,8 @@
             active, jnp.concatenate([history, gated_rows], axis=0)[block_rows:], history
         )
         moments = lax.psum(
-            (jnp.sum(convolved, axis=1), jnp.sum(convolved * convolved, axis=1)), ("fs", "tp")
+            lax.psum((jnp.sum(convolved, axis=1), jnp.sum(convolved * convolved, axis=1)), "fs"),
+            "tp",
         )
         row_mean = moments[0][:, None] / model_width
         row_var = moments[1][:, None] / model_width - row_mean * row_mean

time: 540 us -> 462 us (0.86)
  blocking collectives: 499 us -> 421 us
    psum x5, blocking collectives: 155 us -> 28.3 us  [process_block(): lax.psum((jnp.sum(convolved, axis=1), jnp.sum(convolved * convolved, axis...]
    psum x0 -> x5, blocking collectives: none -> 47.9 us  [process_block(): lax.psum(lax.psum((jnp.sum(convolved, axis=1), jnp.sum(convolved * convol...]
where the time goes in v1:
time: 462 us; the launch traced here: 461 us
  blocking collectives  421 us (91%)
  starting transfers between devices  20.3 us (4%)
  waiting for transfers between devices  7.87 us (2%)
  matrix products  6.46 us (1%)
    all_gather x5, blocking collectives, process_block(): shard_piece = lax.all_gather(normed, ('fs', 'tp'), axis=1, tiled=True)  174 us
    psum x5, blocking collectives, process_block(): squares = lax.psum(jnp.sum(stream_f * stream_f, axis=1), ('fs', 'tp'))  157 us
    psum x5, blocking collectives, process_block(): lax.psum(lax.psum((jnp.sum(convolved, axis=1), jnp.sum(convolved * convol...  47.9 us
    psum x5, blocking collectives, process_block(): lax.psum((jnp.sum(convolved, axis=1), jnp.sum(convolved * convolved, axis...  28.3 us
    ppermute x5, starting transfers between devices, from_behind(): return lax.ppermute(block, axis, route)  20.3 us
  transfers between devices with their start and end apart: 5, of which 5 were waited for; matrix products, arithmetic and copies ran while one was open for 0% of the time, Pallas kernels for 0%

profile of v1, /device:TPU:0, one launch (start us, length us, event | category | flops | bytes accessed | tf_op | source)
XLA Modules:
  0.0 460.7 jit_solution(15233752507512994884)
XLA Ops:
  0.0 6.3 %all_gather.13 = bf16[512,128]{1,0:T(8,128)(2,1)S(1)} all-gather(bf16[256,128]{1,0:T(8,128)(2,1)} %param.13), channel_id=1, replica_groups=mesh['pp'=2,'fs'=4,'tp'=4] {'pp'}, dimensions={0}, use_global_device_ids=true | all-gather | bytes 196608 | tf_op jit(solution)/shard_map/all_gather | solution.py:23
  6.3 0.6 copy-done.1
  7.0 445.3 %while.20 = (s32[]{:T(128)}, bf16[128,128]{1,0:T(8,128)(2,1)S(1)}, f32[30,128]{1,0:T(8,128)S(1)}, bf16[512,128]{1,0:T(8,128)(2,1)S(1)}, s32[]{:T(128)}, /*index=...) while((s32[]{:T(128)}, bf16[128,128]{1,0:T(8,128)(2,1)S(1)}, ...), condition=%wide.region_13.14_spmd.clone, body=%wide.region_0.13_spmd.clone.sunk | while | flops 136180240 | bytes 5905606 | solution.py:109
  7.1 33.1 %psum.76 = f32[128]{0:T(128)S(1)} all-reduce(f32[128]{0:T(128)S(1)} %get-tuple-element.558), channel_id=1, replica_groups=mesh['pp'=2,'fs'=4,'tp'=4] {'fs','tp'}, use_global_device_ids=true, to_apply=%region_2.2 | all-reduce | flops 128 | bytes 1024 | tf_op jit(solution)/shard_map/while/body/eval_jaxpr/psum | solution.py:52
  40.3 33.2 %all_gather.16 = bf16[128,2048]{1,0:T(8,128)(2,1)S(1)} all-gather(bf16[128,128]{1,0:T(8,128)(2,1)S(1)} %fusion.106), channel_id=1, replica_groups=mesh['pp'=2,'fs'=4,'tp'=4] {'fs','tp'}, dimensions={1}, use_global_device_ids=true | all-gather | bytes 557056 | tf_op jit(solution)/shard_map/while/body/eval_jaxpr/all_gather | solution.py:55
  73.5 1.6 conditional.6
  73.5 1.3 fusion
  74.9 0.3 fusion.97
  75.2 0.3 conditional.7
  75.3 0.2 fusion.5
  75.5 0.1 fusion.107
  75.6 5.7 %all-reduce.4 = (f32[128]{0:T(128)S(1)}, f32[128]{0:T(128)S(1)}) all-reduce(f32[128]{0:T(128)S(1)} %get-tuple-element.562, f32[128]{0:T(128)S(1)} %get-tuple-element.563), channel_id=1, replica_groups=mesh['pp'=2,'fs'=4,'tp'=4] {'fs'}, use_global_device_ids=true, to_apply=%region_11.11 | all-reduce | flops 256 | bytes 2048 | tf_op jit(solution)/shard_map/while/body/eval_jaxpr/psum | solution.py:73
  81.3 10.1 %all-reduce.5 = (f32[128]{0:T(128)S(1)}, f32[128]{0:T(128)S(1)}) all-reduce(f32[128]{0:T(128)S(1)} %get-tuple-element.564, f32[128]{0:T(128)S(1)} %get-tuple-element.565), channel_id=1, replica_groups=mesh['pp'=2,'fs'=4,'tp'=4] {'tp'}, use_global_device_ids=true, to_apply=%region_12.12 | all-reduce | flops 256 | bytes 2048 | tf_op jit(solution)/shard_map/while/body/eval_jaxpr/psum | solution.py:72
  91.4 0.1 select_dynamic-update-slice_fusion.2
  91.6 1.6 collective-permute-start
  93.2 1.6 collective-permute-done
  94.9 29.9 %psum.76 = f32[128]{0:T(128)S(1)} all-reduce(f32[128]{0:T(128)S(1)} %get-tuple-element.558), channel_id=1, replica_groups=mesh['pp'=2,'fs'=4,'tp'=4] {'fs','tp'}, use_global_device_ids=true, to_apply=%region_2.2 | all-reduce | flops 128 | bytes 1024 | tf_op jit(solution)/shard_map/while/body/eval_jaxpr/psum | solution.py:52
  124.8 36.9 %all_gather.16 = bf16[128,2048]{1,0:T(8,128)(2,1)S(1)} all-gather(bf16[128,128]{1,0:T(8,128)(2,1)S(1)} %fusion.106), channel_id=1, replica_groups=mesh['pp'=2,'fs'=4,'tp'=4] {'fs','tp'}, dimensions={1}, use_global_device_ids=true | all-gather | bytes 557056 | tf_op jit(solution)/shard_map/while/body/eval_jaxpr/all_gather | solution.py:55
  161.7 1.6 conditional.6
  161.7 1.3 fusion
  163.0 0.3 fusion.97
  163.4 0.3 conditional.7
  163.4 0.2 fusion.5
  163.7 0.1 fusion.107
  163.8 5.7 %all-reduce.4 = (f32[128]{0:T(128)S(1)}, f32[128]{0:T(128)S(1)}) all-reduce(f32[128]{0:T(128)S(1)} %get-tuple-element.562, f32[128]{0:T(128)S(1)} %get-tuple-element.563), channel_id=1, replica_groups=mesh['pp'=2,'fs'=4,'tp'=4] {'fs'}, use_global_device_ids=true, to_apply=%region_11.11 | all-reduce | flops 256 | bytes 2048 | tf_op jit(solution)/shard_map/while/body/eval_jaxpr/psum | solution.py:73
  169.4 8.4 %all-reduce.5 = (f32[128]{0:T(128)S(1)}, f32[128]{0:T(128)S(1)}) all-reduce(f32[128]{0:T(128)S(1)} %get-tuple-element.564, f32[128]{0:T(128)S(1)} %get-tuple-element.565), channel_id=1, replica_groups=mesh['pp'=2,'fs'=4,'tp'=4] {'tp'}, use_global_device_ids=true, to_apply=%region_12.12 | all-reduce | flops 256 | bytes 2048 | tf_op jit(solution)/shard_map/while/body/eval_jaxpr/psum | solution.py:72
  177.8 0.1 select_dynamic-update-slice_fusion.2
  178.0 4.2 collective-permute-start
  182.2 1.6 collective-permute-done
  183.9 31.8 %psum.76 = f32[128]{0:T(128)S(1)} all-reduce(f32[128]{0:T(128)S(1)} %get-tuple-element.558), channel_id=1, replica_groups=mesh['pp'=2,'fs'=4,'tp'=4] {'fs','tp'}, use_global_device_ids=true, to_apply=%region_2.2 | all-reduce | flops 128 | bytes 1024 | tf_op jit(solution)/shard_map/while/body/eval_jaxpr/psum | solution.py:52
  215.8 33.5 %all_gather.16 = bf16[128,2048]{1,0:T(8,128)(2,1)S(1)} all-gather(bf16[128,128]{1,0:T(8,128)(2,1)S(1)} %fusion.106), channel_id=1, replica_groups=mesh['pp'=2,'fs'=4,'tp'=4] {'fs','tp'}, dimensions={1}, use_global_device_ids=true | all-gather | bytes 557056 | tf_op jit(solution)/shard_map/while/body/eval_jaxpr/all_gather | solution.py:55
  249.3 1.6 conditional.6
  249.3 1.3 fusion
  250.6 0.3 fusion.97
  251.0 0.3 conditional.7
  251.0 0.2 fusion.5
  251.3 0.1 fusion.107
  251.4 5.7 %all-reduce.4 = (f32[128]{0:T(128)S(1)}, f32[128]{0:T(128)S(1)}) all-reduce(f32[128]{0:T(128)S(1)} %get-tuple-element.562, f32[128]{0:T(128)S(1)} %get-tuple-element.563), channel_id=1, replica_groups=mesh['pp'=2,'fs'=4,'tp'=4] {'fs'}, use_global_device_ids=true, to_apply=%region_11.11 | all-reduce | flops 256 | bytes 2048 | tf_op jit(solution)/shard_map/while/body/eval_jaxpr/psum | solution.py:73
  257.1 10.7 %all-reduce.5 = (f32[128]{0:T(128)S(1)}, f32[128]{0:T(128)S(1)}) all-reduce(f32[128]{0:T(128)S(1)} %get-tuple-element.564, f32[128]{0:T(128)S(1)} %get-tuple-element.565), channel_id=1, replica_groups=mesh['pp'=2,'fs'=4,'tp'=4] {'tp'}, use_global_device_ids=true, to_apply=%region_12.12 | all-reduce | flops 256 | bytes 2048 | tf_op jit(solution)/shard_map/while/body/eval_jaxpr/psum | solution.py:72
  267.7 0.1 select_dynamic-update-slice_fusion.2
  267.9 4.2 collective-permute-start
  272.1 1.6 collective-permute-done
  273.8 29.8 %psum.76 = f32[128]{0:T(128)S(1)} all-reduce(f32[128]{0:T(128)S(1)} %get-tuple-element.558), channel_id=1, replica_groups=mesh['pp'=2,'fs'=4,'tp'=4] {'fs','tp'}, use_global_device_ids=true, to_apply=%region_2.2 | all-reduce | flops 128 | bytes 1024 | tf_op jit(solution)/shard_map/while/body/eval_jaxpr/psum | solution.py:52
  303.7 36.5 %all_gather.16 = bf16[128,2048]{1,0:T(8,128)(2,1)S(1)} all-gather(bf16[128,128]{1,0:T(8,128)(2,1)S(1)} %fusion.106), channel_id=1, replica_groups=mesh['pp'=2,'fs'=4,'tp'=4] {'fs','tp'}, dimensions={1}, use_global_device_ids=true | all-gather | bytes 557056 | tf_op jit(solution)/shard_map/while/body/eval_jaxpr/all_gather | solution.py:55
  340.2 1.6 conditional.6
  340.2 1.3 fusion
  341.6 0.3 fusion.97
  341.9 0.3 conditional.7
  342.0 0.2 fusion.5
  342.2 0.1 fusion.107
  342.3 5.7 %all-reduce.4 = (f32[128]{0:T(128)S(1)}, f32[128]{0:T(128)S(1)}) all-reduce(f32[128]{0:T(128)S(1)} %get-tuple-element.562, f32[128]{0:T(128)S(1)} %get-tuple-element.563), channel_id=1, replica_groups=mesh['pp'=2,'fs'=4,'tp'=4] {'fs'}, use_global_device_ids=true, to_apply=%region_11.11 | all-reduce | flops 256 | bytes 2048 | tf_op jit(solution)/shard_map/while/body/eval_jaxpr/psum | solution.py:73
  348.0 8.4 %all-reduce.5 = (f32[128]{0:T(128)S(1)}, f32[128]{0:T(128)S(1)}) all-reduce(f32[128]{0:T(128)S(1)} %get-tuple-element.564, f32[128]{0:T(128)S(1)} %get-tuple-element.565), channel_id=1, replica_groups=mesh['pp'=2,'fs'=4,'tp'=4] {'tp'}, use_global_device_ids=true, to_apply=%region_12.12 | all-reduce | flops 256 | bytes 2048 | tf_op jit(solution)/shard_map/while/body/eval_jaxpr/psum | solution.py:72
  356.3 0.1 select_dynamic-update-slice_fusion.2
  356.5 4.2 collective-permute-start
  360.7 1.6 collective-permute-done
  362.4 31.8 %psum.76 = f32[128]{0:T(128)S(1)} all-reduce(f32[128]{0:T(128)S(1)} %get-tuple-element.558), channel_id=1, replica_groups=mesh['pp'=2,'fs'=4,'tp'=4] {'fs','tp'}, use_global_device_ids=true, to_apply=%region_2.2 | all-reduce | flops 128 | bytes 1024 | tf_op jit(solution)/shard_map/while/body/eval_jaxpr/psum | solution.py:52
  394.4 33.8 %all_gather.16 = bf16[128,2048]{1,0:T(8,128)(2,1)S(1)} all-gather(bf16[128,128]{1,0:T(8,128)(2,1)S(1)} %fusion.106), channel_id=1, replica_groups=mesh['pp'=2,'fs'=4,'tp'=4] {'fs','tp'}, dimensions={1}, use_global_device_ids=true | all-gather | bytes 557056 | tf_op jit(solution)/shard_map/while/body/eval_jaxpr/all_gather | solution.py:55
  428.4 5.7 %all-reduce.4 = (f32[128]{0:T(128)S(1)}, f32[128]{0:T(128)S(1)}) all-reduce(f32[128]{0:T(128)S(1)} %get-tuple-element.562, f32[128]{0:T(128)S(1)} %get-tuple-element.563), channel_id=1, replica_groups=mesh['pp'=2,'fs'=4,'tp'=4] {'fs'}, use_global_device_ids=true, to_apply=%region_11.11 | all-reduce | flops 256 | bytes 2048 | tf_op jit(solution)/shard_map/while/body/eval_jaxpr/psum | solution.py:73
  434.0 10.4 %all-reduce.5 = (f32[128]{0:T(128)S(1)}, f32[128]{0:T(128)S(1)}) all-reduce(f32[128]{0:T(128)S(1)} %get-tuple-element.564, f32[128]{0:T(128)S(1)} %get-tuple-element.565), channel_id=1, replica_groups=mesh['pp'=2,'fs'=4,'tp'=4] {'tp'}, use_global_device_ids=true, to_apply=%region_12.12 | all-reduce | flops 256 | bytes 2048 | tf_op jit(solution)/shard_map/while/body/eval_jaxpr/psum | solution.py:72
  444.5 0.1 select_dynamic-update-slice_fusion.2
  444.6 6.1 %collective-permute-start = (bf16[128,128]{1,0:T(8,128)(2,1)S(1)}, bf16[128,128]{1,0:T(8,128)(2,1)S(1)}, u32[]{:S(2)}, u32[]{:S(2)}) collective-permute-start(bf16[128,128]{1,0:T(8,128)(2,1)S(1)} %get-tuple-element.570), channel_id=1, source_target_pairs={{0,16},{1,17},{2,18},{3,19},{4,20},{5,21},{6,22},{7,23},{8,24},{9,... | collective-permute-start | bytes 98312 | tf_op jit(solution)/shard_map/while/body/eval_jaxpr/ppermute | solution.py:14
  450.7 1.6 collective-permute-done
  452.3 7.8 %all_to_all.5 = bf16[2,256,128]{2,1,0:T(8,128)(2,1)S(1)} all-to-all(bf16[2,256,128]{2,1,0:T(8,128)(2,1)S(1)} %bitcast.83), channel_id=1, replica_groups=mesh['pp'=2,'fs'=4,'tp'=4] {'pp'}, dimensions={0} | all-to-all | bytes 262144 | tf_op jit(solution)/shard_map/all_to_all | solution.py:112
  460.1 0.6 slice_bitcast_fusion.31
  (70 shorter events, 1.6 us)
Async XLA Ops:
  0.0 6.3 %copy-start.3 = (bf16[1,31,128]{2,1,0:T(8,128)(2,1)S(1)}, bf16[1,31,128]{2,1,0:T(8,128)(2,1)}, u32[]{:S(2)}) copy-start(bf16[1,31,128]{2,1,0:T(8,128)(2,1)} %param.17) | copy-start | bytes 23812
  6.3 0.7 copy-start.1
  6.3 0.7 copy-start.2
  6.3 0.7 copy-start.4
  7.0 66.5 %copy-start = (bf16[2048,128]{1,0:T(8,128)(2,1)S(1)}, bf16[2048,128]{1,0:T(8,128)(2,1)}, u32[]{:S(2)}) copy-start(bf16[2048,128]{1,0:T(8,128)(2,1)} %get-tuple-element.625) | copy-start | bytes 1572868 | tf_op jit(solution)/shard_map/while
  91.6 3.2 collective-permute-start
  94.7 67.0 %copy-start = (bf16[2048,128]{1,0:T(8,128)(2,1)S(1)}, bf16[2048,128]{1,0:T(8,128)(2,1)}, u32[]{:S(2)}) copy-start(bf16[2048,128]{1,0:T(8,128)(2,1)} %get-tuple-element.625) | copy-start | bytes 1572868 | tf_op jit(solution)/shard_map/while
  178.0 5.8 %collective-permute-start = (bf16[128,128]{1,0:T(8,128)(2,1)S(1)}, bf16[128,128]{1,0:T(8,128)(2,1)S(1)}, u32[]{:S(2)}, u32[]{:S(2)}) collective-permute-start(bf16[128,128]{1,0:T(8,128)(2,1)S(1)} %get-tuple-element.570), channel_id=1, source_target_pairs={{0,16},{1,17},{2,18},{3,19},{4,20},{5,21},{6,22},{7,23},{8,24},{9,... | collective-permute-start | bytes 98312 | tf_op jit(solution)/shard_map/while/body/eval_jaxpr/ppermute | solution.py:14
  183.8 65.5 %copy-start = (bf16[2048,128]{1,0:T(8,128)(2,1)S(1)}, bf16[2048,128]{1,0:T(8,128)(2,1)}, u32[]{:S(2)}) copy-start(bf16[2048,128]{1,0:T(8,128)(2,1)} %get-tuple-element.625) | copy-start | bytes 1572868 | tf_op jit(solution)/shard_map/while
  267.9 5.8 %collective-permute-start = (bf16[128,128]{1,0:T(8,128)(2,1)S(1)}, bf16[128,128]{1,0:T(8,128)(2,1)S(1)}, u32[]{:S(2)}, u32[]{:S(2)}) collective-permute-start(bf16[128,128]{1,0:T(8,128)(2,1)S(1)} %get-tuple-element.570), channel_id=1, source_target_pairs={{0,16},{1,17},{2,18},{3,19},{4,20},{5,21},{6,22},{7,23},{8,24},{9,... | collective-permute-start | bytes 98312 | tf_op jit(solution)/shard_map/while/body/eval_jaxpr/ppermute | solution.py:14
  273.7 66.6 %copy-start = (bf16[2048,128]{1,0:T(8,128)(2,1)S(1)}, bf16[2048,128]{1,0:T(8,128)(2,1)}, u32[]{:S(2)}) copy-start(bf16[2048,128]{1,0:T(8,128)(2,1)} %get-tuple-element.625) | copy-start | bytes 1572868 | tf_op jit(solution)/shard_map/while
  356.5 5.8 %collective-permute-start = (bf16[128,128]{1,0:T(8,128)(2,1)S(1)}, bf16[128,128]{1,0:T(8,128)(2,1)S(1)}, u32[]{:S(2)}, u32[]{:S(2)}) collective-permute-start(bf16[128,128]{1,0:T(8,128)(2,1)S(1)} %get-tuple-element.570), channel_id=1, source_target_pairs={{0,16},{1,17},{2,18},{3,19},{4,20},{5,21},{6,22},{7,23},{8,24},{9,... | collective-permute-start | bytes 98312 | tf_op jit(solution)/shard_map/while/body/eval_jaxpr/ppermute | solution.py:14
  362.3 65.8 %copy-start = (bf16[2048,128]{1,0:T(8,128)(2,1)S(1)}, bf16[2048,128]{1,0:T(8,128)(2,1)}, u32[]{:S(2)}) copy-start(bf16[2048,128]{1,0:T(8,128)(2,1)} %get-tuple-element.625) | copy-start | bytes 1572868 | tf_op jit(solution)/shard_map/while
  444.6 7.7 %collective-permute-start = (bf16[128,128]{1,0:T(8,128)(2,1)S(1)}, bf16[128,128]{1,0:T(8,128)(2,1)S(1)}, u32[]{:S(2)}, u32[]{:S(2)}) collective-permute-start(bf16[128,128]{1,0:T(8,128)(2,1)S(1)} %get-tuple-element.570), channel_id=1, source_target_pairs={{0,16},{1,17},{2,18},{3,19},{4,20},{5,21},{6,22},{7,23},{8,24},{9,... | collective-permute-start | bytes 98312 | tf_op jit(solution)/shard_map/while/body/eval_jaxpr/ppermute | solution.py:14
